TPU v7x, 32 devices: a whole 2x2x4 slice. The times are simulated.
32 devices in a mesh: grp: 2 (over y), ep: 4 (over z), tp: 4 (over x, core).
Axes of the slice: x: 2, y: 2, z: 4, core: 2. Of those that a mesh axis runs over, the one named last changes fastest.
Arguments:
- queries: bfloat16 [3072, 1024], P(('grp', 'ep'), 'tp'), parts along dimension 0, may hold values from -6 to 6
- key_values: bfloat16 [3072, 512], P(('grp', 'ep'), 'tp'), parts along dimension 0, may hold values from -6 to 6
- query_gain: float32 [64], replicated, may hold values from 0.5 to 5
- key_gain: float32 [64], replicated, may hold values from 0.5 to 5
- out_weight: bfloat16 [1024, 2048], P('tp'), may hold values from -0.1875 to 0.1875
- second_batch: bfloat16 [4096, 2048], P(('grp', 'ep', 'tp')), parts along dimension 0, may hold values from -6 to 6
- norm_gain: float32 [2048], replicated, may hold values from 0.1 to 1.9
- routes: int32 [4096, 2], P(('grp', 'ep', 'tp')), parts along dimension 0, may hold values from 0 to 7, all different within a row; in each aligned block of 128 rows (0 to 127, 128 to 255, ...) at most 48 rows name the same one
- route_weights: float32 [4096, 2], P(('grp', 'ep', 'tp')), parts along dimension 0, may hold values from 0.2 to 1
- expert_gate: bfloat16 [8, 2048, 1024], P('ep', None, 'tp'), may hold values from -0.125 to 0.125
- expert_up: bfloat16 [8, 2048, 1024], P('ep', None, 'tp'), may hold values from -0.125 to 0.125
- expert_down: bfloat16 [8, 1024, 2048], P('ep', 'tp'), may hold values from -0.1875 to 0.1875
- shared_gate: bfloat16 [2048, 512], P(None, 'tp'), may hold values from -0.125 to 0.125
- shared_up: bfloat16 [2048, 512], P(None, 'tp'), may hold values from -0.125 to 0.125
- shared_down: bfloat16 [512, 2048], P('tp'), may hold values from -0.25 to 0.25
Outputs:
- mixer_out: bfloat16 [3072, 2048], P(('grp', 'ep', 'tp')), parts along dimension 0
- channel_out: bfloat16 [4096, 2048], P(('grp', 'ep', 'tp')), parts along dimension 0
There are 2 independent parts, one for each index of `grp`. A program takes and returns all parts, laid end to end along the dimension named above; an argument that names none is the same for every part. Nothing has to cross between parts.
Inputs may be any that keep to these rules, and one draw needn't show every extreme that they name: `routes`: each row names 2 different experts. Among the rows of one device no expert is named more than 48 times, and in every draw some expert is named exactly 48 times by the rows of some device.
All inputs are finite; a program needn't handle non-finite values.
Results may differ from a plain program's by a relative error of at most 0.015.
The roundings to bfloat16 on the way count: a program that leaves them out, or rounds other values in their place, can miss the bound.
Values may be sent and summed in bfloat16 or wider, within the bound.
A program may use at most 128 MiB of HBM per device.

v0:
```python
import jax
import jax.numpy as jnp
from jax import lax
from jax.sharding import PartitionSpec as P

GRID_W = 64
rope_base = 10000.0
norm_eps = 1e-06


def head_norm(vectors, gain):
    return (
        vectors * lax.rsqrt(jnp.mean(vectors * vectors, axis=-1, keepdims=True) + norm_eps) * gain
    )


def turn_heads(vectors, positions):
    row_count, head_count, head_size = vectors.shape
    half_size = head_size // 2
    inverse = rope_base ** (-jnp.arange(0, half_size, 2, dtype=jnp.float32) / half_size)
    grid_row = (positions // GRID_W).astype(jnp.float32)
    grid_column = (positions % GRID_W).astype(jnp.float32)
    angles = jnp.concatenate([grid_row[:, None] * inverse, grid_column[:, None] * inverse], axis=-1)
    cosine = jnp.cos(angles)[:, None, :]
    sine = jnp.sin(angles)[:, None, :]
    paired = vectors.reshape(row_count, head_count, half_size, 2)
    first = paired[..., 0]
    second = paired[..., 1]
    turned = jnp.stack([first * cosine - second * sine, first * sine + second * cosine], axis=-1)
    return turned.reshape(vectors.shape)


def slot_ids(route_rows, expert_count, capacity):
    row_count, top_count = route_rows.shape
    flat_routes = route_rows.reshape(-1)
    onehot = (flat_routes[:, None] == jnp.arange(expert_count, dtype=jnp.int32)[None, :]).astype(
        jnp.int32
    )
    earlier = jnp.cumsum(onehot, axis=0) - onehot
    within = jnp.sum(earlier * onehot, axis=1)
    return (flat_routes * capacity + within).reshape(row_count, top_count)


def slot_table(slots, slot_count):
    row_count, top_count = slots.shape
    flat_slots = slots.reshape(-1)
    owner_row = jnp.arange(row_count * top_count, dtype=jnp.int32) // top_count
    matches = flat_slots[None, :] == jnp.arange(slot_count, dtype=jnp.int32)[:, None]
    occupied = jnp.any(matches, axis=1)
    source_row = jnp.sum(jnp.where(matches, owner_row[None, :], 0), axis=1)
    return jnp.where(occupied, source_row, row_count)


def pick_block(row_count):
    for candidate in range(min(row_count, 1024), 0, -1):
        if row_count % candidate == 0:
            return candidate
    return row_count


def attend_keys(query_turned, scale, running, pieces):
    head_size = query_turned.shape[-1]
    key_block = pick_block(pieces.shape[0])
    blocks = pieces.reshape(pieces.shape[0] // key_block, key_block, 2 * head_size)

    def one_block(carried, block_rows):
        top_now, total_now, acc_now = carried
        scores = (
            jnp.einsum(
                "qhd,kd->hqk",
                query_turned,
                block_rows[:, :head_size],
                preferred_element_type=jnp.float32,
            )
            * scale
        )
        top_new = jnp.maximum(top_now, jnp.max(scores, axis=-1))
        shrink = jnp.exp(top_now - top_new)
        exps = jnp.exp(scores - top_new[..., None])
        total_new = total_now * shrink + jnp.sum(exps, axis=-1)
        acc_new = acc_now * shrink[..., None] + jnp.einsum(
            "hqk,kd->hqd",
            exps.astype(jnp.bfloat16),
            block_rows[:, head_size:],
            preferred_element_type=jnp.float32,
        )
        return ((top_new, total_new, acc_new), None)

    result, ignored = lax.scan(one_block, running, blocks)
    return result


def shared_hidden_of(token_rows, gate_weights, up_weights):
    gate_part = jnp.dot(token_rows, gate_weights, preferred_element_type=jnp.float32)
    up_part = jnp.dot(token_rows, up_weights, preferred_element_type=jnp.float32)
    return (jax.nn.silu(gate_part) * up_part).astype(jnp.bfloat16)


def expert_hidden(slot_rows, gate_weights, up_weights):
    gate_part = jnp.einsum(
        "osjcd,jdf->osjcf", slot_rows, gate_weights, preferred_element_type=jnp.float32
    )
    up_part = jnp.einsum(
        "osjcd,jdf->osjcf", slot_rows, up_weights, preferred_element_type=jnp.float32
    )
    return (jax.nn.silu(gate_part) * up_part).astype(jnp.bfloat16)


def body(
    queries,
    key_values,
    query_gain,
    key_gain,
    out_weight,
    second_batch,
    norm_gain,
    routes,
    route_weights,
    expert_gate,
    expert_up,
    expert_down,
    shared_gate,
    shared_up,
    shared_down,
):
    query_rows = queries.shape[0]
    head_size = query_gain.shape[0]
    heads_here = queries.shape[1] // head_size
    ep_count = lax.axis_size("ep")
    positions = lax.axis_index("ep") * query_rows + jnp.arange(query_rows, dtype=jnp.int32)
    query_turned = turn_heads(
        head_norm(
            queries.reshape(query_rows, heads_here, head_size).astype(jnp.float32), query_gain
        ),
        positions,
    ).astype(jnp.bfloat16)
    key_turned = turn_heads(
        head_norm(key_values[:, None, :head_size].astype(jnp.float32), key_gain), positions
    ).astype(jnp.bfloat16)
    keys_and_values = jnp.concatenate([key_turned[:, 0, :], key_values[:, head_size:]], axis=1)
    start_state = (
        jnp.full((heads_here, query_rows), -1e30, jnp.float32),
        jnp.zeros((heads_here, query_rows), jnp.float32),
        jnp.zeros((heads_here, query_rows, head_size), jnp.float32),
    )
    top_all, total_all, acc_all = attend_keys(
        query_turned,
        head_size ** (-0.5),
        start_state,
        lax.all_gather(keys_and_values, "ep", axis=0, tiled=True),
    )
    head_out = (
        (acc_all / total_all[..., None])
        .transpose(1, 0, 2)
        .reshape(query_rows, heads_here * head_size)
        .astype(jnp.bfloat16)
    )
    tok_count = second_batch.shape[0]
    model_width = second_batch.shape[1]
    top_count = routes.shape[1]
    local_experts = expert_gate.shape[0]
    expert_count = local_experts * ep_count
    capacity = 3 * tok_count * top_count // (2 * expert_count)
    slot_count = expert_count * capacity
    token_float = second_batch.astype(jnp.float32)
    normed = (
        token_float
        * lax.rsqrt(jnp.mean(token_float * token_float, axis=-1, keepdims=True) + norm_eps)
        * norm_gain
    ).astype(jnp.bfloat16)
    own_slots = slot_ids(routes, expert_count, capacity)
    shared_hidden = shared_hidden_of(
        lax.all_gather(normed, "tp", axis=0, tiled=True), shared_gate, shared_up
    )
    outgoing = jnp.take(
        normed, slot_table(own_slots, slot_count), axis=0, mode="fill", fill_value=0
    )[None]
    arrived = lax.all_to_all(outgoing, "ep", split_axis=1, concat_axis=1, tiled=True)
    arrived = arrived.reshape(arrived.shape[0], ep_count, local_experts, capacity, model_width)
    hidden = expert_hidden(
        lax.all_gather(arrived, "tp", axis=0, tiled=True), expert_gate, expert_up
    )
    routed_part = jnp.einsum(
        "osjcf,jfd->osjcd", hidden, expert_down, preferred_element_type=jnp.float32
    ).reshape(-1, model_width)
    shared_part = jnp.dot(shared_hidden, shared_down, preferred_element_type=jnp.float32)
    head_partial = jnp.dot(head_out, out_weight, preferred_element_type=jnp.float32)
    attn_sum, routed_sum, shared_sum = (
        lax.psum_scatter(
            head_partial.astype(jnp.bfloat16), "tp", scatter_dimension=0, tiled=True
        ).astype(jnp.float32),
        lax.psum_scatter(
            routed_part.astype(jnp.bfloat16), "tp", scatter_dimension=0, tiled=True
        ).astype(jnp.float32),
        lax.psum_scatter(
            shared_part.astype(jnp.bfloat16), "tp", scatter_dimension=0, tiled=True
        ).astype(jnp.float32),
    )
    returned = lax.all_to_all(
        routed_sum.astype(jnp.bfloat16), "ep", split_axis=0, concat_axis=0, tiled=True
    )
    combined = shared_sum
    for slot_pick in range(top_count):
        combined = combined + route_weights[:, slot_pick : slot_pick + 1] * jnp.take(
            returned, own_slots[:, slot_pick], axis=0
        ).astype(jnp.float32)
    return (attn_sum.astype(jnp.bfloat16), combined.astype(jnp.bfloat16))


def solution(mesh):
    placed = (
        P(("grp", "ep"), "tp"),
        P(("grp", "ep"), "tp"),
        P(),
        P(),
        P("tp", None),
        P(("grp", "ep", "tp"), None),
        P(),
        P(("grp", "ep", "tp"), None),
        P(("grp", "ep", "tp"), None),
        P("ep", None, "tp"),
        P("ep", None, "tp"),
        P("ep", "tp", None),
        P(None, "tp"),
        P(None, "tp"),
        P("tp", None),
    )
    return jax.shard_map(
        body,
        mesh=mesh,
        in_specs=placed,
        out_specs=(P(("grp", "ep", "tp"), None), P(("grp", "ep", "tp"), None)),
        check_vma=False,
    )
```

profile of v0, /device:TPU:0, one launch (start us, length us, event | category | flops | bytes accessed | tf_op | source)
XLA Modules:
  0.0 293.0 jit_solution(5934166044517611856)
XLA Ops:
  7.2 0.9 copy.85
  8.4 0.6 reduce-window.6
  9.0 0.2 slice_reduce_fusion
  9.8 1.2 fusion.25
  11.0 1.2 fusion.27
  12.2 3.1 %gather_fusion = bf16[384,2048]{1,0:T(8,128)(2,1)} fusion(bf16[128,2048]{1,0:T(8,128)(2,1)S(1)} %fusion.27, s32[1024]{0:T(1024)S(1)} %pad_clamp_fusion.2), kind=kCustom, calls=%fused_computation.2 | custom fusion | bytes 3147264 | tf_op jit(solution)/shard_map/jit(_take)/gather | solution.py:175
  15.4 1.6 bitcast_select_fusion
  17.0 4.1 %copy.106 = bf16[1,384,2048]{2,0,1:T(2,128)(2,1)} copy(bf16[1,384,2048]{2,1,0:T(8,128)(2,1)S(1)} %bitcast_select_fusion) | data formatting | bytes 3145728 | tf_op jit(solution)/shard_map/jit(_take)/select_n | solution.py:175
  21.0 0.5 broadcast.414
  21.5 12.4 %reduce.6 = bf16[384,2048]{1,0:T(8,128)(2,1)} reduce(bf16[384,1,2048]{2,1,0:T(2,128)(2,1)} %bitcast.138, bf16[]{:T(256)} %broadcast.414), dimensions={1}, to_apply=%bitcast.118.reduce_sub_computation | reduce | bytes 3145730
  33.9 4.1 %reshape.479 = bf16[4,2,98304]{2,1,0:T(2,128)(2,1)} reshape(bf16[384,2048]{1,0:T(8,128)(2,1)} %reduce.6) | data formatting | bytes 3145728
  38.0 43.4 %all_to_all.17 = bf16[4,2,98304]{2,1,0:T(2,128)(2,1)} all-to-all(bf16[4,2,98304]{2,1,0:T(2,128)(2,1)} %reshape.479), channel_id=1, replica_groups=mesh['grp'=2,'ep'=4,'tp'=4] {'ep'}, dimensions={0} | all-to-all | bytes 3145728 | tf_op jit(solution)/shard_map/all_to_all | solution.py:178
  81.4 4.5 %reshape.480 = bf16[384,1,2048]{2,1,0:T(2,128)(2,1)} reshape(bf16[4,2,98304]{2,1,0:T(2,128)(2,1)} %all_to_all.17) | data formatting | bytes 3145728
  85.9 2.8 copy.96
  88.7 1.3 copy.89
  90.1 0.7 all-gather.3.cloned.1.call-update
  90.9 44.9 %all-gather.5.cloned.1.call-done = bf16[4,4,2,48,2048]{4,3,1,0,2:T(8,128)(2,1)} async-done(((bf16[1,4,2,48,2048]{4,3,1,0,2:T(8,128)(2,1)}), bf16[4,4,2,48,2048]{4,3,1,0,2:T(8,128)(2,1)}) %all-gather.5.cloned.1.call-update) | async-done | bytes 6291472 | tf_op jit(solution)/shard_map/all_gather | solution.py:181
  135.7 6.4 %fusion.14 = f32[2,4,4,48,256]{4,3,2,1,0:T(8,128)} fusion(bf16[4,4,2,48,2048]{4,3,1,0,2:T(8,128)(2,1)} %all-gather.5.cloned.1.call-done, bf16[2,2048,256]{2,1,0:T(8,128)(2,1)} %param.28), kind=kOutput, calls=%fused_computation.26 | convolution fusion | flops 1610612736 | bytes 9961472 | tf_op jit(solution)/shard_map/osjcd,jdf->osjcf/dot_general | solution.py:100
  142.1 10.7 %convert_bitcast_fusion = bf16[4,4,2,48,2048]{4,3,1,0,2:T(8,128)(2,1)} fusion(bf16[2,256,2048]{2,1,0:T(8,128)(2,1)S(1)} %copy-done, f32[2,4,4,48,256]{4,3,2,1,0:T(8,128)} %fusion.14, bf16[4,4,2,48,2048]{4,3,1,0,2:T(8,128)(2,1)} %all-gather.5.cloned.1.call-done, bf16[2,2048,256]{2,1,0:T(8,128)(2,1)} %param.29), kind=kOutput, calls=%fused_computation.20 | convolution fusion | flops 3226730496 | bytes 18350080 | tf_op jit(solution)/shard_map/osjcf,jfd->osjcd/dot_general | solution.py:183
  152.9 6.6 %copy.90 = bf16[4,4,2,48,2048]{4,3,2,1,0:T(8,128)(2,1)} copy(bf16[4,4,2,48,2048]{4,3,1,0,2:T(8,128)(2,1)} %convert_bitcast_fusion) | data formatting | bytes 12582912 | tf_op jit(solution)/shard_map/convert_element_type | solution.py:193
  159.5 0.8 copy-done.9
  161.7 0.2 subtract_convert_fusion.1
  161.9 0.2 multiply_multiply_fusion
  162.2 0.5 subtract_convert_fusion
  162.7 2.4 fusion.57
  165.2 4.9 %convolution_convert_fusion = bf16[512,2048]{1,0:T(8,128)(2,1)} fusion(bf16[128,2048]{1,0:T(8,128)(2,1)} %param.33, bf16[512,2048]{1,0:T(8,128)(2,1)S(1)} %copy-done.5, bf16[2048,128]{1,0:T(8,128)(2,1)} %param.32, f32[512,128]{1,0:T(8,128)S(1)} %fusion.57), kind=kOutput, calls=%fused_computation.21 | convolution fusion | flops 538312704 | bytes 5505024 | tf_op jit(solution)/shard_map/dot_general | solution.py:186
  170.1 0.3 reduce-scatter.4.cloned.1.call-start
  170.3 0.4 pad_maximum_fusion
  171.1 14.6 %all_gather.9 = bf16[1536,128]{0,1:T(8,128)(2,1)S(1)} all-gather(bf16[384,128]{0,1:T(8,128)(2,1)S(1)} %pad_maximum_fusion.1), channel_id=1, replica_groups=mesh['grp'=2,'ep'=4,'tp'=4] {'ep'}, dimensions={0}, use_global_device_ids=true | all-gather | bytes 491520 | tf_op jit(solution)/shard_map/all_gather | solution.py:150
  185.7 0.2 copy.82
  185.9 15.9 %while.15 = (s32[]{:T(128)}, f32[4,384]{1,0:T(4,128)S(1)}, f32[4,384]{1,0:T(4,128)S(1)}, f32[4,384,64]{1,2,0:T(8,128)S(1)}, bf16[2,768,128]{2,1,0:T(8,128)(2,1)S...) while((s32[]{:T(128)}, f32[4,384]{1,0:T(4,128)S(1)}, f32[4,384]{1,0:T(4,128)S(1)}, ...), condition=%wide.region_5.6_spmd.clone, body=%wide.region_2.5_spmd.clone.sunk | while | flops 311729664 | bytes 35094656 | solution.py:89
  186.1 3.0 %bitcast_reduce_fusion.3 = (f32[4,384]{1,0:T(4,128)S(1)}, f32[768,384,4]{1,0,2:T(8,128)}) fusion(bf16[384,4,64]{0,2,1:T(8,128)(2,1)S(1)} %get-tuple-element.203, bf16[768,128]{0,1:T(8,128)(2,1)S(1)} %bitcast.136), kind=kOutput, calls=%fused_computation.4.clone.1 | convolution fusion | flops 153352704 | bytes 5019648 | tf_op jit(solution)/shard_map/while/body/eval_jaxpr/qhd,kd->hqk/dot_general | solution.py:69
  189.1 3.3 %fusion.75 = f32[4,384]{1,0:T(4,128)S(1)} fusion(f32[768,384,4]{1,0,2:T(8,128)} %get-tuple-element.179, f32[4,384]{1,0:T(4,128)S(1)} %select_maximum_fusion.2), kind=kLoop, calls=%fused_computation.7.clone.1 | loop fusion | flops 3537408 | bytes 4730880 | tf_op jit(solution)/shard_map/while/body/eval_jaxpr/reduce_sum | solution.py:80
  192.4 0.5 copy-done.2
  192.9 1.0 fusion.77
  194.1 3.0 %bitcast_reduce_fusion.3 = (f32[4,384]{1,0:T(4,128)S(1)}, f32[768,384,4]{1,0,2:T(8,128)}) fusion(bf16[384,4,64]{0,2,1:T(8,128)(2,1)S(1)} %get-tuple-element.203, bf16[768,128]{0,1:T(8,128)(2,1)S(1)} %bitcast.136), kind=kOutput, calls=%fused_computation.4.clone.1 | convolution fusion | flops 153352704 | bytes 5019648 | tf_op jit(solution)/shard_map/while/body/eval_jaxpr/qhd,kd->hqk/dot_general | solution.py:69
  197.1 3.3 %fusion.75 = f32[4,384]{1,0:T(4,128)S(1)} fusion(f32[768,384,4]{1,0,2:T(8,128)} %get-tuple-element.179, f32[4,384]{1,0:T(4,128)S(1)} %select_maximum_fusion.2), kind=kLoop, calls=%fused_computation.7.clone.1 | loop fusion | flops 3537408 | bytes 4730880 | tf_op jit(solution)/shard_map/while/body/eval_jaxpr/reduce_sum | solution.py:80
  200.4 0.5 copy-done.2
  200.8 1.0 fusion.77
  201.9 1.8 convolution_convert_fusion.1
  203.7 18.2 %reduce-scatter.8.cloned.1.call-done = bf16[384,2048]{1,0:T(8,128)(2,1)} async-done(((bf16[1536,2048]{1,0:T(8,128)(2,1)}), bf16[384,2048]{1,0:T(8,128)(2,1)}) %reduce-scatter.8.cloned.1.call-update) | async-done | bytes 1572880 | tf_op jit(solution)/shard_map/reduce_scatter | solution.py:192
  221.9 4.6 %all-to-all-start.1 = ((bf16[4,96,2048]{2,1,0:T(8,128)(2,1)}), bf16[4,96,2048]{2,1,0:T(8,128)(2,1)S(1)}, u32[]{:S(2)}, u32[]{:S(2)}) async-start(bf16[4,96,2048]{2,1,0:T(8,128)(2,1)} %bitcast.142), calls=%async_computation.4 | async-start | bytes 3145728 | tf_op jit(solution)/shard_map/all_to_all | solution.py:199
  226.8 36.5 %all-to-all-done.1 = bf16[4,96,2048]{2,1,0:T(8,128)(2,1)S(1)} async-done(((bf16[4,96,2048]{2,1,0:T(8,128)(2,1)}), bf16[4,96,2048]{2,1,0:T(8,128)(2,1)S(1)}, u32[]{:S(2)}, u32[]{:S(2)}) %all-to-all-start.1) | async-done | bytes 1572896 | tf_op jit(solution)/shard_map/all_to_all | solution.py:199
  263.3 0.9 gather_fusion.1
  264.2 0.3 copy-done.4
  264.5 3.4 %gather_fusion.2 = bf16[128,2048]{1,0:T(8,128)(2,1)S(1)} fusion(bf16[384,2048]{1,0:T(8,128)(2,1)} %bitcast.134, s32[1024]{0:T(1024)S(1)} %get-tuple-element.135), kind=kCustom, calls=%fused_computation.1.clone | custom fusion | bytes 1049088 | tf_op jit(solution)/shard_map/jit(_take)/gather | solution.py:204
  267.9 2.3 add_convert_fusion
  270.2 16.3 %reduce-scatter.4.cloned.1.call-done = bf16[96,2048]{1,0:T(8,128)(2,1)} async-done(((bf16[384,2048]{1,0:T(8,128)(2,1)}), bf16[96,2048]{1,0:T(8,128)(2,1)}) %reduce-scatter.4.cloned.1.call-update) | async-done | bytes 393232 | tf_op jit(solution)/shard_map/reduce_scatter | solution.py:189
  (91 shorter events, 3.3 us)
Async XLA Ops:
  7.2 135.0 %copy-start = (bf16[2,256,2048]{2,1,0:T(8,128)(2,1)S(1)}, bf16[2,256,2048]{2,1,0:T(8,128)(2,1)}, u32[]{:S(2)}) copy-start(bf16[2,256,2048]{2,1,0:T(8,128)(2,1)} %param.30) | copy-start | bytes 6291460
  7.2 128.6 %all-gather.5.cloned.1.call-start = ((), (), s32[]{:S(2)}) async-start(), calls=%async_computation.8 | async-start | bytes 7864320 | tf_op jit(solution)/shard_map/all_gather | solution.py:181
  12.2 3.1 %copy-start.3 = (bf16[128,2048]{1,0:T(8,128)(2,1)}, bf16[128,2048]{1,0:T(8,128)(2,1)S(1)}, u32[]{:S(2)}) copy-start(bf16[128,2048]{1,0:T(8,128)(2,1)S(1)} %fusion.27) | copy-start | bytes 1572868
  90.1 72.6 %all-gather.3.cloned.1.call-start = ((), (), s32[]{:S(2)}) async-start(), calls=%async_computation.6 | async-start | bytes 2621440 | tf_op jit(solution)/shard_map/all_gather | solution.py:173
  90.8 131.1 %reduce-scatter.8.cloned.1.call-start = ((), (), s32[]{:S(2)}) async-start(), calls=%async_computation.9 | async-start | bytes 7864320 | tf_op jit(solution)/shard_map/reduce_scatter | solution.py:192
  159.4 0.9 copy-start.9
  159.5 1.3 copy-start.13
  159.5 1.4 copy-start.8
  159.5 1.7 copy-start.12
  159.5 108.4 %reduce-scatter.6.cloned.1.call-start = ((), (), s32[]{:S(2)}) async-start(), calls=%async_computation.7 | async-start | bytes 2621440 | tf_op jit(solution)/shard_map/reduce_scatter | solution.py:195
  160.5 2.2 copy-start.7
  162.7 2.5 copy-start.5
  170.1 116.4 %reduce-scatter.4.cloned.1.call-start = ((), (), s32[]{:S(2)}) async-start(), calls=%async_computation.5 | async-start | bytes 1966080 | tf_op jit(solution)/shard_map/reduce_scatter | solution.py:189
  185.9 16.0 %copy-start.6 = (bf16[256,2048]{1,0:T(8,128)(2,1)S(1)}, bf16[256,2048]{1,0:T(8,128)(2,1)}, u32[]{:S(2)}) copy-start(bf16[256,2048]{1,0:T(8,128)(2,1)} %param.23) | copy-start | bytes 3145732
  189.1 3.8 %copy-start.2 = (f32[768,384,4]{1,0,2:T(8,128)S(1)}, f32[768,384,4]{1,0,2:T(8,128)}, u32[]{:S(2)}) copy-start(f32[768,384,4]{1,0,2:T(8,128)} %get-tuple-element.179) | copy-start | bytes 14155780 | tf_op jit(solution)/shard_map/while
  197.1 3.8 %copy-start.2 = (f32[768,384,4]{1,0,2:T(8,128)S(1)}, f32[768,384,4]{1,0,2:T(8,128)}, u32[]{:S(2)}) copy-start(f32[768,384,4]{1,0,2:T(8,128)} %get-tuple-element.179) | copy-start | bytes 14155780 | tf_op jit(solution)/shard_map/while
  203.7 23.0 %copy-start.10 = (s32[128,2]{0,1:T(2,128)S(1)}, s32[128,2]{0,1:T(2,128)}, u32[]{:S(2)}) copy-start(s32[128,2]{0,1:T(2,128)} %param.26) | copy-start | bytes 3076
  203.7 23.1 %copy-start.11 = (f32[128,2]{0,1:T(2,128)S(1)}, f32[128,2]{0,1:T(2,128)}, u32[]{:S(2)}) copy-start(f32[128,2]{0,1:T(2,128)} %param.27) | copy-start | bytes 3076
  221.9 41.4 %all-to-all-start.1 = ((bf16[4,96,2048]{2,1,0:T(8,128)(2,1)}), bf16[4,96,2048]{2,1,0:T(8,128)(2,1)S(1)}, u32[]{:S(2)}, u32[]{:S(2)}) async-start(bf16[4,96,2048]{2,1,0:T(8,128)(2,1)} %bitcast.142), calls=%async_computation.4 | async-start | bytes 3145728 | tf_op jit(solution)/shard_map/all_to_all | solution.py:199
  263.3 1.2 copy-start.4
  264.5 22.0 %copy-start.1 = (bf16[2,256,2048]{2,1,0:T(8,128)(2,1)S(1)}, bf16[2,256,2048]{2,1,0:T(8,128)(2,1)}, u32[]{:S(2)}) copy-start(bf16[2,256,2048]{2,1,0:T(8,128)(2,1)} %param.30) | copy-start | bytes 6291460
Sparse Core Ops, SparseCore 0:
  90.2 45.4 all-gather.4
  137.9 22.5 all-gather.2
  163.0 58.8 reduce-scatter.7
  224.3 31.1 reduce-scatter.5
  258.4 28.0 reduce-scatter.3
where the time goes:
time: 294 us; the launch traced here: 293 us
  waiting for transfers between devices  117 us (40%)
  blocking collectives  58 us (20%)
  local copies, waits for them, and re-layouts  36.6 us (12%)
  matrix products  34.1 us (12%)
  other arithmetic  28.3 us (10%)
  between operations  14.2 us (5%)
  starting transfers between devices  5.02 us (2%)
    all_gather x1, waiting for transfers between devices, body(): lax.all_gather(arrived, 'tp', axis=0, tiled=True)  44.9 us
    all_to_all x1, blocking collectives, body(): lax.all_to_all(outgoing, 'ep', split_axis=1, concat_axis=1, tiled=True)  43.4 us
    all_to_all x1, waiting for transfers between devices, body(): lax.all_to_all(routed_sum.astype(jnp.bfloat16), 'ep', split_axis=0, conca...  36.5 us
    reduce_scatter x1, waiting for transfers between devices, body(): lax.psum_scatter(routed_part.astype(jnp.bfloat16), 'tp', scatter_dimensio...  18.2 us
    reduce_scatter x1, waiting for transfers between devices, body(): lax.psum_scatter(head_partial.astype(jnp.bfloat16), 'tp', scatter_dimensi...  16.3 us
    all_gather x1, blocking collectives, body(): lax.all_gather(keys_and_values, 'ep', axis=0, tiled=True)  14.6 us
    unnamed x34, local copies, waits for them, and re-layouts  14.3 us
    unnamed x4, other arithmetic  12.4 us
  transfers between devices with their start and end apart: 6, of which 4 were waited for; matrix products, arithmetic and copies ran while one was open for 20% of the time, Pallas kernels for 0%

commit v1 on v0

--- a/solution.py
+++ b/solution.py
@@ -175,7 +175,10 @@
     outgoing = jnp.take(
         normed, slot_table(own_slots, slot_count), axis=0, mode="fill", fill_value=0
     )[None]
-    arrived = lax.all_to_all(outgoing, "ep", split_axis=1, concat_axis=1, tiled=True)
+    arrived = jnp.concatenate(
+        lax.all_to_all(jnp.stack(jnp.split(outgoing, lax.axis_size("ep"), axis=1)), "ep", 0, 0),
+        axis=1,
+    )
     arrived = arrived.reshape(arrived.shape[0], ep_count, local_experts, capacity, model_width)
     hidden = expert_hidden(
         lax.all_gather(arrived, "tp", axis=0, tiled=True), expert_gate, expert_up

time: 294 us -> 265 us (0.901)
  local copies, waits for them, and re-layouts: 36.6 us -> 23 us
  other arithmetic: 28.3 us -> 16.1 us
  waiting for transfers between devices: 117 us -> 113 us
    unnamed x4 -> x3, other arithmetic: 12.4 us -> 0.01 us
    unnamed x34 -> x24, local copies, waits for them, and re-layouts: 14.3 us -> 2.24 us
    select_n x1 -> x0, local copies, waits for them, and re-layouts: 4.05 us -> none  [body(): jnp.take(normed, slot_table(own_slots, slot_count), axis=0, mode='fill',...]
  transfers between devices with their start and end apart: 6 -> 6, of which waited for: 4 -> 4; matrix products, arithmetic and copies ran while one was open for 20% -> 23% of each run, Pallas kernels for 0% -> 0%
where the time goes in v1:
time: 265 us
  waiting for transfers between devices  113 us (43%)
  blocking collectives  57.7 us (22%)
  matrix products  35.9 us (14%)
  local copies, waits for them, and re-layouts  23 us (9%)
  other arithmetic  16.1 us (6%)
  between operations  14.2 us (5%)
  starting transfers between devices  4.98 us (2%)
    all_gather x1, waiting for transfers between devices, body(): lax.all_gather(arrived, 'tp', axis=0, tiled=True)  44.9 us
    all_to_all x1, blocking collectives, body(): lax.all_to_all(jnp.stack(jnp.split(outgoing, lax.axis_size('ep'), axis=1)...  43.1 us
    all_to_all x1, waiting for transfers between devices, body(): lax.all_to_all(routed_sum.astype(jnp.bfloat16), 'ep', split_axis=0, conca...  36.6 us
    reduce_scatter x1, waiting for transfers between devices, body(): lax.psum_scatter(routed_part.astype(jnp.bfloat16), 'tp', scatter_dimensio...  15.9 us
    reduce_scatter x1, waiting for transfers between devices, body(): lax.psum_scatter(head_partial.astype(jnp.bfloat16), 'tp', scatter_dimensi...  14.6 us
    all_gather x1, blocking collectives, body(): lax.all_gather(keys_and_values, 'ep', axis=0, tiled=True)  14.6 us
    dot_general x1, matrix products, body(): jnp.einsum('osjcf,jfd->osjcd', hidden, expert_down, preferred_element_typ...  10.7 us
    convert_element_type x1, local copies, waits for them, and re-layouts, body(): routed_part.astype(jnp.bfloat16)  6.59 us
  transfers between devices with their start and end apart: 6, of which 4 were waited for; matrix products, arithmetic and copies ran while one was open for 23% of the time, Pallas kernels for 0%

profile of v1, /device:TPU:0, one launch (start us, length us, event | category | flops | bytes accessed | tf_op | source)
XLA Modules:
  0.0 264.7 jit_solution(9451065103485733270)
XLA Ops:
  7.2 0.9 copy.70
  8.4 0.6 reduce-window.6
  9.0 0.2 slice_reduce_fusion
  9.4 0.2 fusion.29
  9.7 1.2 fusion.25
  11.0 1.2 fusion.27
  12.2 3.1 %gather_fusion = bf16[384,2048]{1,0:T(8,128)(2,1)} fusion(bf16[128,2048]{1,0:T(8,128)(2,1)S(1)} %fusion.27, s32[1024]{0:T(1024)S(1)} %pad_clamp_fusion.2), kind=kCustom, calls=%fused_computation.2 | custom fusion | bytes 3147264 | tf_op jit(solution)/shard_map/jit(_take)/gather | solution.py:175
  15.4 1.6 bitcast_select_fusion
  17.1 0.2 pad_maximum_fusion
  17.3 43.1 %all_to_all.17 = bf16[4,1,96,2048]{3,2,1,0:T(8,128)(2,1)S(1)} all-to-all(bf16[4,1,96,2048]{3,2,1,0:T(8,128)(2,1)S(1)} %pad_maximum_fusion), channel_id=1, replica_groups=mesh['grp'=2,'ep'=4,'tp'=4] {'ep'}, dimensions={0} | all-to-all | bytes 3145728 | tf_op jit(solution)/shard_map/all_to_all | solution.py:179
  60.4 1.2 copy.73
  61.7 0.7 all-gather.3.cloned.1.call-update
  62.5 44.9 %all-gather.5.cloned.1.call-done = bf16[4,4,2,48,2048]{4,3,1,0,2:T(8,128)(2,1)} async-done(((bf16[1,4,2,48,2048]{4,3,1,0,2:T(8,128)(2,1)}), bf16[4,4,2,48,2048]{4,3,1,0,2:T(8,128)(2,1)}) %all-gather.5.cloned.1.call-update) | async-done | bytes 6291472 | tf_op jit(solution)/shard_map/all_gather | solution.py:184
  107.3 6.4 %fusion.14 = f32[2,4,4,48,256]{4,3,2,1,0:T(8,128)} fusion(bf16[4,4,2,48,2048]{4,3,1,0,2:T(8,128)(2,1)} %all-gather.5.cloned.1.call-done, bf16[2,2048,256]{2,1,0:T(8,128)(2,1)} %param.28), kind=kOutput, calls=%fused_computation.26 | convolution fusion | flops 1610612736 | bytes 9961472 | tf_op jit(solution)/shard_map/osjcd,jdf->osjcf/dot_general | solution.py:100
  113.7 10.7 %convert_bitcast_fusion = bf16[4,4,2,48,2048]{4,3,1,0,2:T(8,128)(2,1)} fusion(bf16[2,256,2048]{2,1,0:T(8,128)(2,1)S(1)} %copy-done, f32[2,4,4,48,256]{4,3,2,1,0:T(8,128)} %fusion.14, bf16[4,4,2,48,2048]{4,3,1,0,2:T(8,128)(2,1)} %all-gather.5.cloned.1.call-done, bf16[2,2048,256]{2,1,0:T(8,128)(2,1)} %param.29), kind=kOutput, calls=%fused_computation.20 | convolution fusion | flops 3226730496 | bytes 18350080 | tf_op jit(solution)/shard_map/osjcf,jfd->osjcd/dot_general | solution.py:186
  124.4 6.6 %copy.74 = bf16[4,4,2,48,2048]{4,3,2,1,0:T(8,128)(2,1)} copy(bf16[4,4,2,48,2048]{4,3,1,0,2:T(8,128)(2,1)} %convert_bitcast_fusion) | data formatting | bytes 12582912 | tf_op jit(solution)/shard_map/convert_element_type | solution.py:196
  131.0 0.2 reduce-scatter.6.cloned.1.call-start
  131.3 0.7 copy-done.6
  131.9 0.2 copy.68
  132.1 0.2 reshape.437
  132.4 0.7 fusion.56
  133.6 0.2 fusion.39
  133.9 0.2 subtract_convert_fusion.1
  134.1 0.2 multiply_multiply_fusion
  134.3 0.5 subtract_convert_fusion
  134.9 2.3 fusion.57
  137.2 5.5 %convolution_convert_fusion = bf16[512,2048]{1,0:T(8,128)(2,1)} fusion(bf16[128,2048]{1,0:T(8,128)(2,1)} %param.33, bf16[512,2048]{1,0:T(8,128)(2,1)} %all-gather.3.cloned.1.call-done, bf16[2048,128]{1,0:T(8,128)(2,1)} %param.32, f32[512,128]{1,0:T(8,128)S(1)} %fusion.57), kind=kOutput, calls=%fused_computation.21 | convolution fusion | flops 538312704 | bytes 5505024 | tf_op jit(solution)/shard_map/dot_general | solution.py:189
  142.7 0.4 pad_maximum_fusion.1
  143.4 0.3 copy-done.5
  143.7 14.6 %all_gather.9 = bf16[1536,128]{0,1:T(8,128)(2,1)S(1)} all-gather(bf16[384,128]{0,1:T(8,128)(2,1)S(1)} %pad_maximum_fusion.2), channel_id=1, replica_groups=mesh['grp'=2,'ep'=4,'tp'=4] {'ep'}, dimensions={0}, use_global_device_ids=true | all-gather | bytes 491520 | tf_op jit(solution)/shard_map/all_gather | solution.py:150
  158.3 0.2 copy.67
  158.5 16.0 %while.15 = (s32[]{:T(128)}, f32[4,384]{1,0:T(4,128)S(1)}, f32[4,384]{1,0:T(4,128)S(1)}, f32[4,384,64]{1,2,0:T(8,128)S(1)}, bf16[2,768,128]{2,1,0:T(8,128)(2,1)S...) while((s32[]{:T(128)}, f32[4,384]{1,0:T(4,128)S(1)}, f32[4,384]{1,0:T(4,128)S(1)}, ...), condition=%wide.region_5.6_spmd.clone, body=%wide.region_2.5_spmd.clone.sunk | while | flops 311729664 | bytes 35094656 | solution.py:89
  158.7 3.0 %bitcast_reduce_fusion.3 = (f32[4,384]{1,0:T(4,128)S(1)}, f32[768,384,4]{1,0,2:T(8,128)}) fusion(bf16[384,4,64]{0,2,1:T(8,128)(2,1)S(1)} %get-tuple-element.201, bf16[768,128]{0,1:T(8,128)(2,1)S(1)} %bitcast.138), kind=kOutput, calls=%fused_computation.4.clone.1 | convolution fusion | flops 153352704 | bytes 5019648 | tf_op jit(solution)/shard_map/while/body/eval_jaxpr/qhd,kd->hqk/dot_general | solution.py:69
  161.8 3.3 %fusion.75 = f32[4,384]{1,0:T(4,128)S(1)} fusion(f32[768,384,4]{1,0,2:T(8,128)} %get-tuple-element.177, f32[4,384]{1,0:T(4,128)S(1)} %select_maximum_fusion.2), kind=kLoop, calls=%fused_computation.7.clone.1 | loop fusion | flops 3537408 | bytes 4730880 | tf_op jit(solution)/shard_map/while/body/eval_jaxpr/reduce_sum | solution.py:80
  165.0 0.5 copy-done.1
  165.5 1.0 fusion.77
  166.7 3.0 %bitcast_reduce_fusion.3 = (f32[4,384]{1,0:T(4,128)S(1)}, f32[768,384,4]{1,0,2:T(8,128)}) fusion(bf16[384,4,64]{0,2,1:T(8,128)(2,1)S(1)} %get-tuple-element.201, bf16[768,128]{0,1:T(8,128)(2,1)S(1)} %bitcast.138), kind=kOutput, calls=%fused_computation.4.clone.1 | convolution fusion | flops 153352704 | bytes 5019648 | tf_op jit(solution)/shard_map/while/body/eval_jaxpr/qhd,kd->hqk/dot_general | solution.py:69
  169.7 3.3 %fusion.75 = f32[4,384]{1,0:T(4,128)S(1)} fusion(f32[768,384,4]{1,0,2:T(8,128)} %get-tuple-element.177, f32[4,384]{1,0:T(4,128)S(1)} %select_maximum_fusion.2), kind=kLoop, calls=%fused_computation.7.clone.1 | loop fusion | flops 3537408 | bytes 4730880 | tf_op jit(solution)/shard_map/while/body/eval_jaxpr/reduce_sum | solution.py:80
  173.0 0.5 copy-done.1
  173.5 1.0 fusion.77
  174.6 3.0 %convolution_convert_fusion.1 = bf16[384,2048]{1,0:T(8,128)(2,1)} fusion(bf16[384,256]{0,1:T(8,128)(2,1)S(1)} %bitcast.143, bf16[256,2048]{1,0:T(8,128)(2,1)} %param.23), kind=kOutput, calls=%fused_computation.22 | convolution fusion | flops 403439616 | bytes 2818048 | tf_op jit(solution)/shard_map/dot_general | solution.py:190
  177.6 15.9 %reduce-scatter.8.cloned.1.call-done = bf16[384,2048]{1,0:T(8,128)(2,1)} async-done(((bf16[1536,2048]{1,0:T(8,128)(2,1)}), bf16[384,2048]{1,0:T(8,128)(2,1)}) %reduce-scatter.8.cloned.1.call-update) | async-done | bytes 1572880 | tf_op jit(solution)/shard_map/reduce_scatter | solution.py:195
  193.5 4.6 %all-to-all-start.1 = ((bf16[4,96,2048]{2,1,0:T(8,128)(2,1)}), bf16[4,96,2048]{2,1,0:T(8,128)(2,1)}, u32[]{:S(2)}, u32[]{:S(2)}) async-start(bf16[4,96,2048]{2,1,0:T(8,128)(2,1)} %bitcast.142), calls=%async_computation.4 | async-start | bytes 3145728 | tf_op jit(solution)/shard_map/all_to_all | solution.py:202
  198.4 36.6 %all-to-all-done.1 = bf16[4,96,2048]{2,1,0:T(8,128)(2,1)} async-done(((bf16[4,96,2048]{2,1,0:T(8,128)(2,1)}), bf16[4,96,2048]{2,1,0:T(8,128)(2,1)}, u32[]{:S(2)}, u32[]{:S(2)}) %all-to-all-start.1) | async-done | bytes 1572896 | tf_op jit(solution)/shard_map/all_to_all | solution.py:202
  235.0 3.1 %gather_fusion.1 = bf16[128,2048]{1,0:T(8,128)(2,1)S(1)} fusion(bf16[384,2048]{1,0:T(8,128)(2,1)} %bitcast.27, s32[1024]{0:T(1024)S(1)} %get-tuple-element.134), kind=kCustom, calls=%fused_computation.clone | custom fusion | bytes 1049088 | tf_op jit(solution)/shard_map/jit(_take)/gather | solution.py:207
  238.1 3.1 %gather_fusion.2 = bf16[128,2048]{1,0:T(8,128)(2,1)S(1)} fusion(bf16[384,2048]{1,0:T(8,128)(2,1)} %bitcast.27, s32[1024]{0:T(1024)S(1)} %get-tuple-element.133), kind=kCustom, calls=%fused_computation.1.clone | custom fusion | bytes 1049088 | tf_op jit(solution)/shard_map/jit(_take)/gather | solution.py:207
  241.2 2.3 add_convert_fusion
  243.5 14.6 %reduce-scatter.4.cloned.1.call-done = bf16[96,2048]{1,0:T(8,128)(2,1)} async-done(((bf16[384,2048]{1,0:T(8,128)(2,1)}), bf16[96,2048]{1,0:T(8,128)(2,1)}) %reduce-scatter.4.cloned.1.call-update) | async-done | bytes 393232 | tf_op jit(solution)/shard_map/reduce_scatter | solution.py:192
  (81 shorter events, 2.6 us)
Async XLA Ops:
  7.2 106.5 %copy-start = (bf16[2,256,2048]{2,1,0:T(8,128)(2,1)S(1)}, bf16[2,256,2048]{2,1,0:T(8,128)(2,1)}, u32[]{:S(2)}) copy-start(bf16[2,256,2048]{2,1,0:T(8,128)(2,1)} %param.30) | copy-start | bytes 6291460
  7.2 100.1 %all-gather.5.cloned.1.call-start = ((), (), s32[]{:S(2)}) async-start(), calls=%async_computation.8 | async-start | bytes 7864320 | tf_op jit(solution)/shard_map/all_gather | solution.py:184
  12.2 3.1 %copy-start.2 = (bf16[128,2048]{1,0:T(8,128)(2,1)}, bf16[128,2048]{1,0:T(8,128)(2,1)S(1)}, u32[]{:S(2)}) copy-start(bf16[128,2048]{1,0:T(8,128)(2,1)S(1)} %fusion.27) | copy-start | bytes 1572868
  61.7 73.2 %all-gather.3.cloned.1.call-start = ((), (), s32[]{:S(2)}) async-start(), calls=%async_computation.6 | async-start | bytes 2621440 | tf_op jit(solution)/shard_map/all_gather | solution.py:173
  62.4 131.1 %reduce-scatter.8.cloned.1.call-start = ((), (), s32[]{:S(2)}) async-start(), calls=%async_computation.9 | async-start | bytes 7864320 | tf_op jit(solution)/shard_map/reduce_scatter | solution.py:195
  131.0 0.9 copy-start.6
  131.0 1.3 copy-start.10
  131.0 1.4 copy-start.4
  131.0 2.3 copy-start.9
  131.0 110.2 %reduce-scatter.6.cloned.1.call-start = ((), (), s32[]{:S(2)}) async-start(), calls=%async_computation.7 | async-start | bytes 2621440 | tf_op jit(solution)/shard_map/reduce_scatter | solution.py:198
  132.1 2.8 %copy-start.3 = (bf16[2048,128]{1,0:T(8,128)(2,1)S(1)}, bf16[2048,128]{1,0:T(8,128)(2,1)}, u32[]{:S(2)}) copy-start(bf16[2048,128]{1,0:T(8,128)(2,1)} %param.31) | copy-start | bytes 1572868
  142.7 1.0 copy-start.5
  142.7 115.4 %reduce-scatter.4.cloned.1.call-start = ((), (), s32[]{:S(2)}) async-start(), calls=%async_computation.5 | async-start | bytes 1966080 | tf_op jit(solution)/shard_map/reduce_scatter | solution.py:192
  161.8 3.8 %copy-start.1 = (f32[768,384,4]{1,0,2:T(8,128)S(1)}, f32[768,384,4]{1,0,2:T(8,128)}, u32[]{:S(2)}) copy-start(f32[768,384,4]{1,0,2:T(8,128)} %get-tuple-element.177) | copy-start | bytes 14155780 | tf_op jit(solution)/shard_map/while
  169.7 3.8 %copy-start.1 = (f32[768,384,4]{1,0,2:T(8,128)S(1)}, f32[768,384,4]{1,0,2:T(8,128)}, u32[]{:S(2)}) copy-start(f32[768,384,4]{1,0,2:T(8,128)} %get-tuple-element.177) | copy-start | bytes 14155780 | tf_op jit(solution)/shard_map/while
  177.6 20.7 %copy-start.7 = (s32[128,2]{0,1:T(2,128)S(1)}, s32[128,2]{0,1:T(2,128)}, u32[]{:S(2)}) copy-start(s32[128,2]{0,1:T(2,128)} %param.26) | copy-start | bytes 3076
  177.6 20.8 %copy-start.8 = (f32[128,2]{0,1:T(2,128)S(1)}, f32[128,2]{0,1:T(2,128)}, u32[]{:S(2)}) copy-start(f32[128,2]{0,1:T(2,128)} %param.27) | copy-start | bytes 3076
  193.5 41.5 %all-to-all-start.1 = ((bf16[4,96,2048]{2,1,0:T(8,128)(2,1)}), bf16[4,96,2048]{2,1,0:T(8,128)(2,1)}, u32[]{:S(2)}, u32[]{:S(2)}) async-start(bf16[4,96,2048]{2,1,0:T(8,128)(2,1)} %bitcast.142), calls=%async_computation.4 | async-start | bytes 3145728 | tf_op jit(solution)/shard_map/all_to_all | solution.py:202
Sparse Core Ops, SparseCore 0:
  61.8 45.4 all-gather.4
  109.5 22.5 all-gather.2
  134.6 58.8 reduce-scatter.7
  195.9 31.1 reduce-scatter.5
  230.0 28.0 reduce-scatter.3
